TPU v7x, 32 devices: a whole 2x2x4 slice. The times are simulated.
32 devices in a mesh: grp: 2 (over y), ep: 8 (over z, x), tp: 2 (over core).
Axes of the slice: x: 2, y: 2, z: 4, core: 2. Of those that a mesh axis runs over, the one named last changes fastest.
Arguments:
- tokens: bfloat16 [4096, 2048], P(('grp', 'ep'), 'tp'), parts along dimension 0, may hold values from -6 to 6
- norm_gain: bfloat16 [2048], P('tp'), may hold values from 0.099609375 to 1.8984375
- w_gate: bfloat16 [8, 2048, 1024], P('ep', None, 'tp'), may hold values from -0.125 to 0.125
- w_up: bfloat16 [8, 2048, 1024], P('ep', None, 'tp'), may hold values from -0.125 to 0.125
- w_down: bfloat16 [8, 1024, 2048], P('ep', 'tp'), may hold values from -0.1875 to 0.1875
- expert_ids: int32 [4096, 2], P(('grp', 'ep')), parts along dimension 0, may hold values from 0 to 7, as said below
- combine: float32 [4096, 2], P(('grp', 'ep')), parts along dimension 0, may hold values from 0.1 to 1
- final_gain: bfloat16 [2048], P('tp'), may hold values from 0.099609375 to 1.8984375
Outputs:
- result: bfloat16 [4096, 2048], P(('grp', 'ep'), 'tp'), parts along dimension 0
There are 2 independent parts, one for each index of `grp`. A program takes and returns all parts, laid end to end along the dimension named above; an argument that names none is the same for every part. Nothing has to cross between parts.
Inputs may be any that keep to these rules, and one draw needn't show every extreme that they name: `expert_ids`: the experts form 4 groups of consecutive ids of equal size; the 2 experts of a row are different and lie in one group. Among the rows of one index of ep no expert is named more than 160 times, and in each such block some expert is named exactly 160 times.
All inputs are finite; a program needn't handle non-finite values.
Results may differ from a plain program's by a relative error of at most 0.0077.
Values may be sent and summed in bfloat16 or wider, within the bound.
A program may use at most 64 MiB of HBM per device.

v0:
```python
import jax
import jax.numpy as jnp
from jax import lax
from jax.sharding import PartitionSpec as P

GROUPS = 4


def body(tokens, norm_gain, w_gate, w_up, w_down, expert_ids, combine, final_gain):
    eps = 1e-06
    tok_dev, half = tokens.shape
    n_ep = lax.axis_size("ep")
    n_tp = lax.axis_size("tp")
    width = half * n_tp
    exp_dev = w_gate.shape[0]
    experts = exp_dev * n_ep
    per_group = experts // GROUPS
    capacity = tok_dev // 8 * 5 * 2 // per_group
    top = expert_ids.shape[1]
    narrow = tokens.astype(jnp.float32)
    squares = lax.psum(jnp.sum(narrow * narrow, axis=1), "tp")
    scale = lax.rsqrt(squares[:, None] / width + eps)
    normed = (narrow * scale * norm_gain.astype(jnp.float32)).astype(jnp.bfloat16)
    columns = normed.shape[1]
    flat = expert_ids.reshape(-1)
    onehot = (flat[:, None] == jnp.arange(experts, dtype=jnp.int32)[None, :]).astype(jnp.int32)
    ranking = jnp.sum(jnp.cumsum(onehot, axis=0) * onehot, axis=1) - 1
    target = flat * capacity + ranking
    sources = jnp.arange(tok_dev * top, dtype=jnp.int32) // top
    owner = jnp.full((experts * capacity,), tok_dev, jnp.int32).at[target].set(sources)
    padded = jnp.concatenate([normed, jnp.zeros((1, columns), jnp.bfloat16)], axis=0)
    outgoing = padded[owner].reshape(n_ep, exp_dev * capacity, columns)
    arrived = lax.all_to_all(outgoing, "ep", split_axis=0, concat_axis=0, tiled=True)
    rows = (
        arrived.reshape(n_ep, exp_dev, capacity, columns)
        .transpose(1, 0, 2, 3)
        .reshape(exp_dev, n_ep * capacity, columns)
    )
    piece = lax.all_gather(rows, "tp", axis=2, tiled=True)
    gate = jnp.einsum("erd,edf->erf", piece, w_gate, preferred_element_type=jnp.float32)
    upper = jnp.einsum("erd,edf->erf", piece, w_up, preferred_element_type=jnp.float32)
    hidden = (jax.nn.silu(gate) * upper).astype(jnp.bfloat16)
    partial_out = jnp.einsum(
        "erf,efd->erd", hidden, w_down, preferred_element_type=jnp.float32
    ).astype(jnp.bfloat16)
    shares = (
        lax.psum_scatter(partial_out, "tp", scatter_dimension=2, tiled=True)
        .astype(jnp.float32)
        .astype(jnp.bfloat16)
    )
    homeward = (
        shares.reshape(exp_dev, n_ep, capacity, half)
        .transpose(1, 0, 2, 3)
        .reshape(n_ep, exp_dev * capacity, half)
    )
    returned = lax.all_to_all(homeward, "ep", split_axis=0, concat_axis=0, tiled=True).reshape(
        experts * capacity, half
    )
    picked = returned[target].astype(jnp.float32).reshape(tok_dev, top, half)
    mixed = jnp.sum(picked * combine[:, :, None], axis=1)
    totals = lax.psum(jnp.sum(mixed * mixed, axis=1), "tp")
    norm = lax.rsqrt(totals[:, None] / width + eps)
    return (mixed * norm * final_gain.astype(jnp.float32)).astype(jnp.bfloat16)


def solution(mesh):
    placed = (
        P(("grp", "ep"), "tp"),
        P("tp"),
        P("ep", None, "tp"),
        P("ep", None, "tp"),
        P("ep", "tp", None),
        P(("grp", "ep"), None),
        P(("grp", "ep"), None),
        P("tp"),
    )
    return jax.shard_map(
        body, mesh=mesh, in_specs=placed, out_specs=P(("grp", "ep"), "tp"), check_vma=False
    )
```

profile of v0, /device:TPU:0, one launch (start us, length us, event | category | flops | bytes accessed | tf_op | source)
XLA Modules:
  0.0 225.1 jit_solution(16053872975609984581)
XLA Ops:
  6.5 1.0 copy.11
  7.5 0.1 eq.29
  7.7 0.1 eq.25
  7.8 0.7 broadcast_multiply_fusion
  8.5 1.1 reduce-window.6
  9.6 0.2 slice_reduce_fusion
  9.9 0.1 fusion.21
  10.0 0.1 copy.10
  10.1 0.1 mul.81
  10.3 2.5 %scatter_custom_fusion = s32[1280]{0:T(1024)S(1)} fusion(s32[512]{0:T(512)S(1)} %bitcast.39, s32[512]{0:T(512)S(1)} %add_select_fusion, s32[]{:T(128)} %constant.38.clone.1), kind=kCustom, calls=%fused_computation.35 | custom fusion | bytes 5124 | tf_op jit(solution)/shard_map/scatter | solution.py:30
  12.8 0.7 convert_element_type.40
  13.5 1.2 fusion.18
  14.7 2.6 %psum.14 = f32[256]{0:T(256)S(1)} all-reduce(f32[256]{0:T(256)S(1)} %fusion.18), channel_id=1, replica_groups=mesh['grp'=2,'ep'=8,'tp'=2] {'tp'}, use_global_device_ids=true, to_apply=%region_1.0 | all-reduce | flops 256 | bytes 2048 | tf_op jit(solution)/shard_map/psum | solution.py:21
  17.3 1.2 fusion.20
  18.6 5.1 %gather_fusion = bf16[1280,1024]{1,0:T(8,128)(2,1)} fusion(bf16[257,1024]{1,0:T(8,128)(2,1)S(1)} %concatenate.3, s32[2048]{0:T(1024)S(1)} %pad_clamp_fusion), kind=kCustom, calls=%fused_computation | custom fusion | bytes 5248000 | tf_op jit(solution)/shard_map/gather | solution.py:32
  23.7 67.0 %all_to_all.10 = bf16[8,160,1024]{2,1,0:T(8,128)(2,1)} all-to-all(bf16[8,160,1024]{2,1,0:T(8,128)(2,1)} %bitcast.37), channel_id=1, replica_groups=mesh['grp'=2,'ep'=8,'tp'=2] {'ep'}, dimensions={0} | all-to-all | bytes 5242880 | tf_op jit(solution)/shard_map/all_to_all | solution.py:33
  90.7 0.0 all-gather.2.cloned.1.call-update
  90.7 0.0 reduce-scatter.2.cloned.1.call-start
  90.8 14.4 %all-gather.2.cloned.1.call-done = bf16[1,1280,2048]{2,1,0:T(8,128)(2,1)} async-done(((bf16[1,1280,1024]{2,1,0:T(8,128)(2,1)}), bf16[1,1280,2048]{2,1,0:T(8,128)(2,1)}) %all-gather.2.cloned.1.call-update) | async-done | bytes 5242896 | tf_op jit(solution)/shard_map/all_gather | solution.py:39
  105.2 7.6 %fusion.3 = f32[1280,512]{1,0:T(8,128)} fusion(bf16[1,1280,2048]{2,1,0:T(8,128)(2,1)} %all-gather.2.cloned.1.call-done, bf16[1,2048,512]{2,1,0:T(8,128)(2,1)} %param.10), kind=kOutput, calls=%fused_computation.7 | convolution fusion | flops 2684354560 | bytes 9961472 | tf_op jit(solution)/shard_map/erd,edf->erf/dot_general | solution.py:40
  112.7 10.3 %fusion = bf16[1,1280,2048]{2,1,0:T(8,128)(2,1)} fusion(bf16[1,512,2048]{2,1,0:T(8,128)(2,1)S(1)} %copy-done, bf16[1,1280,2048]{2,1,0:T(8,128)(2,1)} %all-gather.2.cloned.1.call-done, f32[1280,512]{1,0:T(8,128)} %fusion.3, bf16[1,2048,512]{2,1,0:T(8,128)(2,1)} %param.11), kind=kOutput, calls=%fused_computation.4 | convolution fusion | flops 5375262720 | bytes 17301504 | tf_op jit(solution)/shard_map/erf,efd->erd/dot_general | solution.py:43
  123.1 0.0 reduce-scatter.2.cloned.1.call-update
  123.1 14.2 %reduce-scatter.2.cloned.1.call-done = bf16[1,1280,1024]{2,1,0:T(8,128)(2,1)} async-done(((bf16[1,1280,2048]{2,1,0:T(8,128)(2,1)}), bf16[1,1280,1024]{2,1,0:T(8,128)(2,1)}) %reduce-scatter.2.cloned.1.call-update) | async-done | bytes 2621456 | tf_op jit(solution)/shard_map/reduce_scatter | solution.py:47
  137.3 6.0 %all-to-all-start.1 = ((bf16[8,160,1024]{2,1,0:T(8,128)(2,1)}), bf16[8,160,1024]{2,1,0:T(8,128)(2,1)}, u32[]{:S(2)}, u32[]{:S(2)}) async-start(bf16[8,160,1024]{2,1,0:T(8,128)(2,1)} %bitcast.38), calls=%async_computation.2 | async-start | bytes 5242880 | tf_op jit(solution)/shard_map/all_to_all | solution.py:56
  143.3 0.1 copy.13
  143.5 59.7 %all-to-all-done.1 = bf16[8,160,1024]{2,1,0:T(8,128)(2,1)} async-done(((bf16[8,160,1024]{2,1,0:T(8,128)(2,1)}), bf16[8,160,1024]{2,1,0:T(8,128)(2,1)}, u32[]{:S(2)}, u32[]{:S(2)}) %all-to-all-start.1) | async-done | bytes 2621472 | tf_op jit(solution)/shard_map/all_to_all | solution.py:56
  203.2 4.8 %gather_fusion.1 = bf16[512,1024]{1,0:T(8,128)(2,1)S(1)} fusion(bf16[1280,1024]{1,0:T(8,128)(2,1)} %bitcast.12, s32[1024]{0:T(1024)S(1)} %pad_clamp_fusion.1), kind=kCustom, calls=%fused_computation.1 | custom fusion | bytes 2099200 | tf_op jit(solution)/shard_map/gather | solution.py:59
  208.0 2.4 %reshape.105 = f32[256,2,1024]{2,1,0:T(2,128)} reshape(bf16[512,1024]{1,0:T(8,128)(2,1)S(1)} %gather_fusion.1) | data formatting | bytes 3145728 | tf_op jit(solution)/shard_map/convert_element_type | solution.py:59
  210.4 4.3 %multiply_reduce_fusion = f32[256,1024]{1,0:T(8,128)S(1)} fusion(f32[256,2,1024]{2,1,0:T(2,128)} %reshape.105, f32[256,2]{1,0:T(8,128)S(1)} %copy.13), kind=kLoop, calls=%fused_computation.14 | loop fusion | flops 786432 | bytes 3147776 | tf_op jit(solution)/shard_map/reduce_sum | solution.py:60
  214.7 0.1 multiply_reduce_fusion.1
  214.8 2.5 %psum.15 = f32[256]{0:T(256)S(1)} all-reduce(f32[256]{0:T(256)S(1)} %multiply_reduce_fusion.1), channel_id=1, replica_groups=mesh['grp'=2,'ep'=8,'tp'=2] {'tp'}, use_global_device_ids=true, to_apply=%region_9.10 | all-reduce | flops 256 | bytes 2048 | tf_op jit(solution)/shard_map/psum | solution.py:61
  217.3 1.0 multiply_convert_fusion
  (20 shorter events, 0.1 us)
Async XLA Ops:
  6.5 106.2 %copy-start = (bf16[1,512,2048]{2,1,0:T(8,128)(2,1)S(1)}, bf16[1,512,2048]{2,1,0:T(8,128)(2,1)}, u32[]{:S(2)}) copy-start(bf16[1,512,2048]{2,1,0:T(8,128)(2,1)} %param.12) | copy-start | bytes 6291460
  6.5 98.6 %all-gather.2.cloned.1.call-start = ((), (), s32[]{:S(2)}) async-start(), calls=%async_computation.3 | async-start | bytes 7864320 | tf_op jit(solution)/shard_map/all_gather | solution.py:39
  90.7 46.6 %reduce-scatter.2.cloned.1.call-start = ((), (), s32[]{:S(2)}) async-start(), calls=%async_computation.4 | async-start | bytes 7864320 | tf_op jit(solution)/shard_map/reduce_scatter | solution.py:47
  137.3 6.0 %copy-start.1 = (f32[256,2]{0,1:T(2,128)S(1)}, f32[256,2]{0,1:T(2,128)}, u32[]{:S(2)}) copy-start(f32[256,2]{0,1:T(2,128)} %param.14) | copy-start | bytes 6148
  137.3 6.2 %copy-start.2 = (bf16[1024]{0:T(1024)(128)(2,1)S(1)}, bf16[1024]{0:T(1024)(128)(2,1)}, u32[]{:S(2)}) copy-start(bf16[1024]{0:T(1024)(128)(2,1)} %param.15) | copy-start | bytes 6148
  137.3 65.9 %all-to-all-start.1 = ((bf16[8,160,1024]{2,1,0:T(8,128)(2,1)}), bf16[8,160,1024]{2,1,0:T(8,128)(2,1)}, u32[]{:S(2)}, u32[]{:S(2)}) async-start(bf16[8,160,1024]{2,1,0:T(8,128)(2,1)} %bitcast.38), calls=%async_computation.2 | async-start | bytes 5242880 | tf_op jit(solution)/shard_map/all_to_all | solution.py:56
Sparse Core Ops, SparseCore 0:
  90.8 14.2 all-gather.1
  123.2 14.0 reduce-scatter.1
where the time goes:
time: 226 us; the launch traced here: 225 us
  waiting for transfers between devices  88.3 us (39%)
  blocking collectives  72.1 us (32%)
  matrix products  17.9 us (8%)
  local copies, waits for them, and re-layouts  16.6 us (7%)
  between operations  13.5 us (6%)
  other arithmetic  10.6 us (5%)
  starting transfers between devices  6.05 us (3%)
    all_to_all x1, blocking collectives, body(): lax.all_to_all(outgoing, 'ep', split_axis=0, concat_axis=0, tiled=True)  67 us
    all_to_all x1, waiting for transfers between devices, body(): lax.all_to_all(homeward, 'ep', split_axis=0, concat_axis=0, tiled=True)  59.7 us
    all_gather x1, waiting for transfers between devices, body(): piece = lax.all_gather(rows, 'tp', axis=2, tiled=True)  14.4 us
    reduce_scatter x1, waiting for transfers between devices, body(): lax.psum_scatter(partial_out, 'tp', scatter_dimension=2, tiled=True)  14.2 us
    dot_general x1, matrix products, body(): jnp.einsum('erf,efd->erd', hidden, w_down, preferred_element_type=jnp.flo...  10.3 us
    dot_general x1, matrix products, body(): jnp.einsum('erd,edf->erf', piece, w_gate, preferred_element_type=jnp.floa...  7.55 us
    all_to_all x1, starting transfers between devices, body(): lax.all_to_all(homeward, 'ep', split_axis=0, concat_axis=0, tiled=True)  6.01 us
    gather x1, local copies, waits for them, and re-layouts, body(): outgoing = padded[owner].reshape(n_ep, exp_dev * capacity, columns)  5.08 us
  transfers between devices with their start and end apart: 3, of which 3 were waited for; matrix products, arithmetic and copies ran while one was open for 0% of the time, Pallas kernels for 0%

commit v1 on v0

--- a/solution.py
+++ b/solution.py
@@ -36,7 +36,7 @@
         .transpose(1, 0, 2, 3)
         .reshape(exp_dev, n_ep * capacity, columns)
     )
-    piece = lax.all_gather(rows, "tp", axis=2, tiled=True)
+    piece = jnp.concatenate(lax.all_gather(rows, axis_name="tp"), axis=2)
     gate = jnp.einsum("erd,edf->erf", piece, w_gate, preferred_element_type=jnp.float32)
     upper = jnp.einsum("erd,edf->erf", piece, w_up, preferred_element_type=jnp.float32)
     hidden = (jax.nn.silu(gate) * upper).astype(jnp.bfloat16)

time: 226 us -> 234 us (1.035)
  local copies, waits for them, and re-layouts: 16.6 us -> 24.6 us
    all_gather x0 -> x1, local copies, waits for them, and re-layouts: none -> 7.91 us  [body(): piece = jnp.concatenate(lax.all_gather(rows, axis_name='tp'), axis=2)]
where the time goes in v1:
time: 234 us; the launch traced here: 233 us
  waiting for transfers between devices  88.4 us (38%)
  blocking collectives  72.1 us (31%)
  local copies, waits for them, and re-layouts  24.6 us (11%)
  matrix products  17.9 us (8%)
  between operations  13.5 us (6%)
  other arithmetic  10.5 us (4%)
  starting transfers between devices  6.04 us (3%)
    all_to_all x1, blocking collectives, body(): lax.all_to_all(outgoing, 'ep', split_axis=0, concat_axis=0, tiled=True)  67 us
    all_to_all x1, waiting for transfers between devices, body(): lax.all_to_all(homeward, 'ep', split_axis=0, concat_axis=0, tiled=True)  59.7 us
    all_gather x1, waiting for transfers between devices, body(): piece = jnp.concatenate(lax.all_gather(rows, axis_name='tp'), axis=2)  14.4 us
    reduce_scatter x1, waiting for transfers between devices, body(): lax.psum_scatter(partial_out, 'tp', scatter_dimension=2, tiled=True)  14.2 us
    dot_general x1, matrix products, body(): jnp.einsum('erf,efd->erd', hidden, w_down, preferred_element_type=jnp.flo...  10.3 us
    all_gather x1, local copies, waits for them, and re-layouts, body(): piece = jnp.concatenate(lax.all_gather(rows, axis_name='tp'), axis=2)  7.91 us
    dot_general x1, matrix products, body(): jnp.einsum('erd,edf->erf', piece, w_gate, preferred_element_type=jnp.floa...  7.58 us
    all_to_all x1, starting transfers between devices, body(): lax.all_to_all(homeward, 'ep', split_axis=0, concat_axis=0, tiled=True)  6 us
  transfers between devices with their start and end apart: 3, of which 3 were waited for; matrix products, arithmetic and copies ran while one was open for 0% of the time, Pallas kernels for 0%

profile of v1, /device:TPU:0, one launch (start us, length us, event | category | flops | bytes accessed | tf_op | source)
XLA Modules:
  0.0 233.1 jit_solution(17328793003309246335)
XLA Ops:
  6.5 1.0 copy.21
  7.5 0.1 eq.29
  7.7 0.1 eq.25
  7.8 0.7 broadcast_multiply_fusion
  8.5 1.1 reduce-window.6
  9.6 0.2 slice_reduce_fusion
  9.9 0.1 fusion.11
  10.0 0.1 copy.20
  10.1 0.1 mul.81
  10.3 2.5 %scatter_custom_fusion = s32[1280]{0:T(1024)S(1)} fusion(s32[512]{0:T(512)S(1)} %bitcast.35, s32[512]{0:T(512)S(1)} %add_select_fusion, s32[]{:T(128)} %constant.38.clone.1), kind=kCustom, calls=%fused_computation.32 | custom fusion | bytes 5124 | tf_op jit(solution)/shard_map/scatter | solution.py:30
  12.8 0.7 convert_element_type.40
  13.5 1.2 fusion.6
  14.7 2.6 %psum.14 = f32[256]{0:T(256)S(1)} all-reduce(f32[256]{0:T(256)S(1)} %fusion.6), channel_id=1, replica_groups=mesh['grp'=2,'ep'=8,'tp'=2] {'tp'}, use_global_device_ids=true, to_apply=%region_1.0 | all-reduce | flops 256 | bytes 2048 | tf_op jit(solution)/shard_map/psum | solution.py:21
  17.3 1.2 fusion.8
  18.6 5.1 %gather_fusion = bf16[1280,1024]{1,0:T(8,128)(2,1)} fusion(bf16[257,1024]{1,0:T(8,128)(2,1)S(1)} %concatenate.3, s32[2048]{0:T(1024)S(1)} %pad_clamp_fusion), kind=kCustom, calls=%fused_computation | custom fusion | bytes 5248000 | tf_op jit(solution)/shard_map/gather | solution.py:32
  23.7 67.0 %all_to_all.10 = bf16[8,160,1024]{2,1,0:T(8,128)(2,1)} all-to-all(bf16[8,160,1024]{2,1,0:T(8,128)(2,1)} %bitcast.31), channel_id=1, replica_groups=mesh['grp'=2,'ep'=8,'tp'=2] {'ep'}, dimensions={0} | all-to-all | bytes 5242880 | tf_op jit(solution)/shard_map/all_to_all | solution.py:33
  90.7 0.0 all-gather.2.cloned.1.call-update
  90.7 0.0 reduce-scatter.2.cloned.1.call-start
  90.8 14.4 %all-gather.2.cloned.1.call-done = bf16[2,1,1280,1024]{3,2,1,0:T(8,128)(2,1)} async-done(((bf16[1,1,1280,1024]{3,2,1,0:T(8,128)(2,1)}), bf16[2,1,1280,1024]{3,2,1,0:T(8,128)(2,1)}) %all-gather.2.cloned.1.call-update) | async-done | bytes 5242896 | tf_op jit(solution)/shard_map/all_gather | solution.py:39
  105.2 7.9 %copy.23 = bf16[2,1,1280,1024]{2,3,0,1:T(8,128)(2,1)} copy(bf16[2,1,1280,1024]{3,2,1,0:T(8,128)(2,1)} %all-gather.2.cloned.1.call-done) | data formatting | bytes 10485760 | tf_op jit(solution)/shard_map/all_gather | solution.py:39
  113.1 7.6 %fusion.4 = f32[1280,512]{1,0:T(8,128)} fusion(bf16[1280,2048]{0,1:T(8,128)(2,1)} %bitcast.32, bf16[1,2048,512]{2,1,0:T(8,128)(2,1)} %param.10), kind=kOutput, calls=%fused_computation.9 | convolution fusion | flops 2684354560 | bytes 9961472 | tf_op jit(solution)/shard_map/erd,edf->erf/dot_general | solution.py:40
  120.7 10.3 %fusion = bf16[1,1280,2048]{2,1,0:T(8,128)(2,1)} fusion(bf16[1,512,2048]{2,1,0:T(8,128)(2,1)S(1)} %copy-done, bf16[1280,2048]{0,1:T(8,128)(2,1)} %bitcast.33, f32[1280,512]{1,0:T(8,128)} %fusion.4, bf16[1,2048,512]{2,1,0:T(8,128)(2,1)} %param.11), kind=kOutput, calls=%fused_computation.4 | convolution fusion | flops 5375262720 | bytes 17301504 | tf_op jit(solution)/shard_map/erf,efd->erd/dot_general | solution.py:43
  131.1 14.2 %reduce-scatter.2.cloned.1.call-done = bf16[1,1280,1024]{2,1,0:T(8,128)(2,1)} async-done(((bf16[1,1280,2048]{2,1,0:T(8,128)(2,1)}), bf16[1,1280,1024]{2,1,0:T(8,128)(2,1)}) %reduce-scatter.2.cloned.1.call-update) | async-done | bytes 2621456 | tf_op jit(solution)/shard_map/reduce_scatter | solution.py:47
  145.3 6.0 %all-to-all-start.1 = ((bf16[8,160,1024]{2,1,0:T(8,128)(2,1)}), bf16[8,160,1024]{2,1,0:T(8,128)(2,1)}, u32[]{:S(2)}, u32[]{:S(2)}) async-start(bf16[8,160,1024]{2,1,0:T(8,128)(2,1)} %bitcast.34), calls=%async_computation.2 | async-start | bytes 5242880 | tf_op jit(solution)/shard_map/all_to_all | solution.py:56
  151.3 0.1 copy.24
  151.4 59.7 %all-to-all-done.1 = bf16[8,160,1024]{2,1,0:T(8,128)(2,1)} async-done(((bf16[8,160,1024]{2,1,0:T(8,128)(2,1)}), bf16[8,160,1024]{2,1,0:T(8,128)(2,1)}, u32[]{:S(2)}, u32[]{:S(2)}) %all-to-all-start.1) | async-done | bytes 2621472 | tf_op jit(solution)/shard_map/all_to_all | solution.py:56
  211.2 4.8 %gather_fusion.1 = bf16[512,1024]{1,0:T(8,128)(2,1)S(1)} fusion(bf16[1280,1024]{1,0:T(8,128)(2,1)} %bitcast.14, s32[1024]{0:T(1024)S(1)} %pad_clamp_fusion.1), kind=kCustom, calls=%fused_computation.1 | custom fusion | bytes 2099200 | tf_op jit(solution)/shard_map/gather | solution.py:59
  216.0 2.4 %reshape.112 = f32[256,2,1024]{2,1,0:T(2,128)} reshape(bf16[512,1024]{1,0:T(8,128)(2,1)S(1)} %gather_fusion.1) | data formatting | bytes 3145728 | tf_op jit(solution)/shard_map/convert_element_type | solution.py:59
  218.4 4.3 %multiply_reduce_fusion = f32[256,1024]{1,0:T(8,128)S(1)} fusion(f32[256,2,1024]{2,1,0:T(2,128)} %reshape.112, f32[256,2]{1,0:T(8,128)S(1)} %copy.24), kind=kLoop, calls=%fused_computation.11 | loop fusion | flops 786432 | bytes 3147776 | tf_op jit(solution)/shard_map/reduce_sum | solution.py:60
  222.7 0.1 multiply_reduce_fusion.1
  222.8 2.5 %psum.15 = f32[256]{0:T(256)S(1)} all-reduce(f32[256]{0:T(256)S(1)} %multiply_reduce_fusion.1), channel_id=1, replica_groups=mesh['grp'=2,'ep'=8,'tp'=2] {'tp'}, use_global_device_ids=true, to_apply=%region_9.10 | all-reduce | flops 256 | bytes 2048 | tf_op jit(solution)/shard_map/psum | solution.py:61
  225.3 1.0 multiply_convert_fusion
  (21 shorter events, 0.2 us)
Async XLA Ops:
  6.5 114.2 %copy-start = (bf16[1,512,2048]{2,1,0:T(8,128)(2,1)S(1)}, bf16[1,512,2048]{2,1,0:T(8,128)(2,1)}, u32[]{:S(2)}) copy-start(bf16[1,512,2048]{2,1,0:T(8,128)(2,1)} %param.12) | copy-start | bytes 6291460
  6.5 98.7 %all-gather.2.cloned.1.call-start = ((), (), s32[]{:S(2)}) async-start(), calls=%async_computation.3 | async-start | bytes 7864320 | tf_op jit(solution)/shard_map/all_gather | solution.py:39
  90.7 54.5 %reduce-scatter.2.cloned.1.call-start = ((), (), s32[]{:S(2)}) async-start(), calls=%async_computation.4 | async-start | bytes 7864320 | tf_op jit(solution)/shard_map/reduce_scatter | solution.py:47
  145.3 6.0 %copy-start.1 = (f32[256,2]{0,1:T(2,128)S(1)}, f32[256,2]{0,1:T(2,128)}, u32[]{:S(2)}) copy-start(f32[256,2]{0,1:T(2,128)} %param.14) | copy-start | bytes 6148
  145.3 6.2 %copy-start.2 = (bf16[1024]{0:T(1024)(128)(2,1)S(1)}, bf16[1024]{0:T(1024)(128)(2,1)}, u32[]{:S(2)}) copy-start(bf16[1024]{0:T(1024)(128)(2,1)} %param.15) | copy-start | bytes 6148
  145.3 65.9 %all-to-all-start.1 = ((bf16[8,160,1024]{2,1,0:T(8,128)(2,1)}), bf16[8,160,1024]{2,1,0:T(8,128)(2,1)}, u32[]{:S(2)}, u32[]{:S(2)}) async-start(bf16[8,160,1024]{2,1,0:T(8,128)(2,1)} %bitcast.34), calls=%async_computation.2 | async-start | bytes 5242880 | tf_op jit(solution)/shard_map/all_to_all | solution.py:56
Sparse Core Ops, SparseCore 0:
  90.9 14.2 all-gather.1
  131.2 14.0 reduce-scatter.1
